TPU v7x, 32 devices: a whole 2x2x4 slice. The times are simulated.
32 devices in a mesh: grp: 2 (over y), kv: 4 (over z), tp: 4 (over x, core).
Axes of the slice: x: 2, y: 2, z: 4, core: 2. Of those that a mesh axis runs over, the one named last changes fastest.
Arguments:
- piece_rows: bfloat16 [512, 2048], P(('grp', 'kv')), parts along dimension 0, may hold values from -6 to 6
- dec_rows: bfloat16 [16, 2048], P(('grp', 'kv')), parts along dimension 0, may hold values from -6 to 6
- norm_gain: float32 [2048], replicated, may hold values from 0.1 to 1.9
- w_query: bfloat16 [2048, 1024], P(None, 'tp'), may hold values from -0.25 to 0.25
- w_key: bfloat16 [2048, 256], P(None, 'tp'), may hold values from -0.125 to 0.125
- w_value: bfloat16 [2048, 256], P(None, 'tp'), may hold values from -0.125 to 0.125
- w_forget: bfloat16 [2048, 16], P(None, 'tp'), may hold values from -0.125 to 0.125
- forget_bias: float32 [16], P('tp'), may hold values from 3 to 12
- piece_decay: float32 [16, 512], P('tp', ('grp', 'kv')), parts along dimension 1, may hold values from -3 to 0
- cache_kv: bfloat16 [6144, 4, 128], P(('grp', 'kv'), 'tp'), parts along dimension 0, may hold values from -150 to 150
- cache_gate: float32 [16, 6144], P('tp', ('grp', 'kv')), parts along dimension 1, may hold values from -156.6 to 0, as said below
- dec_cache: bfloat16 [16, 3072, 4, 128], P(('grp', 'kv'), None, 'tp'), parts along dimension 0, may hold values from -150 to 150
- dec_gate: float32 [16, 16, 3072], P(('grp', 'kv'), 'tp'), parts along dimension 0, may hold values from -156.6 to 0, as said below
- dec_lengths: int32 [16], P(('grp', 'kv')), parts along dimension 0, may hold values from 1 to 3072, as said below
- w_out: bfloat16 [1024, 2048], P(None, 'tp'), may hold values from -0.75 to 0.75
Outputs:
- piece_out: bfloat16 [512, 2048], P(('grp', 'kv'), 'tp'), parts along dimension 0
- dec_out: bfloat16 [16, 2048], P(('grp', 'kv'), 'tp'), parts along dimension 0
There are 2 independent parts, one for each index of `grp`. A program takes and returns all parts, laid end to end along the dimension named above; an argument that names none is the same for every part. Nothing has to cross between parts.
Inputs may be any that keep to these rules, and one draw needn't show every extreme that they name: `cache_gate`: each head's values never fall from one position to the next and are 0 at the last cached position. `dec_gate`: each sequence's and head's values never rise from one position to the next. Sequence b's cache holds its first dec_lengths[b] positions; in each part some sequence holds 3072.
All inputs are finite; a program needn't handle non-finite values.
Results may differ from a plain program's by a relative error of at most 0.006.
The roundings to bfloat16 on the way count: a program that leaves them out, or rounds other values in their place, can miss the bound.
Values may be sent and summed in bfloat16 or wider, within the bound.
A program may use at most 64 MiB of HBM per device.

v0:
```python
import jax
import jax.numpy as jnp
from jax import lax
from jax.sharding import PartitionSpec as P


def carried_in(array, axis, combine, identity):
    length, mine = (lax.axis_size(axis), lax.axis_index(axis))
    everything = lax.all_gather(array, axis)
    start = jnp.broadcast_to(jnp.asarray(identity, array.dtype), array.shape)

    def lap(k, before):
        reached = k < mine
        new = combine(before, everything[k])
        return jnp.where(reached, new, before)

    return lax.fori_loop(0, length, lap, start)


def norm_rows(rows, gain):
    wide = rows.astype(jnp.float32)
    scale = lax.rsqrt(jnp.mean(wide * wide, axis=-1, keepdims=True) + 1e-06)
    return (wide * scale * gain).astype(jnp.bfloat16)


def add_terms(earlier, later):
    return earlier + later


def merge_state(state, part):
    peak, total, numer = state
    new_peak, new_total, new_numer = part
    highest = jnp.maximum(peak, new_peak)
    keep = jnp.exp(peak - highest)
    fresh = jnp.exp(new_peak - highest)
    return (
        highest,
        total * keep + new_total * fresh,
        numer * keep[..., None] + new_numer * fresh[..., None],
    )


def group_partial(query, query_index, group_kv, group_bias, group, past_rows, new_rows):
    head_width = query.shape[-1]
    keys = group_kv[..., :head_width]
    values = group_kv[..., head_width:]
    score = jnp.einsum("bkgd,nkd->bkgn", query, keys, preferred_element_type=jnp.float32)
    score = score * head_width ** (-0.5) + group_bias[None]
    rank = jnp.arange(group_kv.shape[0], dtype=jnp.int32)
    new_index = group * new_rows + rank - past_rows
    visible = (rank < past_rows)[None, :] | (new_index[None, :] <= query_index[:, None])
    score = jnp.where(visible[:, None, None, :], score, -jnp.inf)
    peak = jnp.max(score, axis=-1)
    weight = jnp.exp(score - peak[..., None])
    total = jnp.sum(weight, axis=-1)
    numer = jnp.einsum(
        "bkgn,nkd->bkgd", weight.astype(jnp.bfloat16), values, preferred_element_type=jnp.float32
    )
    return (peak, total, numer)


def decode_attention(query, new_key, new_value, new_gate, cache, gate, lengths):
    seqs, pairs_here, group_size, head_width = query.shape
    span = cache.shape[1]
    keys = cache[..., :head_width]
    values = cache[..., head_width:]
    target_location = jnp.arange(span, dtype=jnp.int32)
    last_gate = jnp.sum(
        jnp.where(target_location[None, None, :] == lengths[:, None, None] - 1, gate, 0.0), axis=-1
    )
    score = jnp.einsum(
        "skgd,slkd->skgl", query, keys, preferred_element_type=jnp.float32
    ) * head_width ** (-0.5)
    score = score - gate.reshape(seqs, pairs_here, group_size, span)
    score = jnp.where(
        (target_location[None, :] < lengths[:, None])[:, None, None, :], score, -jnp.inf
    )
    own = jnp.einsum(
        "skgd,skd->skg", query, new_key, preferred_element_type=jnp.float32
    ) * head_width ** (-0.5)
    own = own - (last_gate + new_gate).reshape(seqs, pairs_here, group_size)
    peak = jnp.maximum(jnp.max(score, axis=-1), own)
    weight = jnp.exp(score - peak[..., None])
    own_weight = jnp.exp(own - peak)
    total = jnp.sum(weight, axis=-1) + own_weight
    numer = jnp.einsum(
        "skgl,slkd->skgd", weight.astype(jnp.bfloat16), values, preferred_element_type=jnp.float32
    )
    numer = numer + own_weight.astype(jnp.bfloat16).astype(jnp.float32)[..., None] * new_value[
        :, :, None, :
    ].astype(jnp.float32)
    return numer / total[..., None]


def local(
    piece_rows,
    dec_rows,
    norm_gain,
    w_query,
    w_key,
    w_value,
    w_forget,
    forget_bias,
    piece_decay,
    cache_kv,
    cache_gate,
    dec_cache,
    dec_gate,
    dec_lengths,
    w_out,
):
    piece_count = piece_rows.shape[0]
    dec_count = dec_rows.shape[0]
    past_rows = cache_kv.shape[0]
    pairs_here = cache_kv.shape[1]
    head_width = cache_kv.shape[2] // 2
    heads_here = w_forget.shape[1]
    group_size = heads_here // pairs_here
    group_rows = past_rows + piece_count
    normed = norm_rows(jnp.concatenate([piece_rows, dec_rows], axis=0), norm_gain)
    query = jnp.dot(normed, w_query, preferred_element_type=jnp.float32).astype(jnp.bfloat16)
    new_key = jnp.dot(normed, w_key, preferred_element_type=jnp.float32).astype(jnp.bfloat16)
    new_value = jnp.dot(normed, w_value, preferred_element_type=jnp.float32).astype(jnp.bfloat16)
    log_gate = jax.nn.log_sigmoid(
        jnp.dot(normed, w_forget, preferred_element_type=jnp.float32) + forget_bias
    )
    piece_gate = log_gate[:piece_count] + piece_decay.T
    running = jnp.cumsum(piece_gate, axis=0)
    before = carried_in(running[-1], "kv", add_terms, jnp.zeros((heads_here,), jnp.float32))
    new_bias = -(running + before[None, :]).T
    piece_kv = jnp.concatenate(
        [
            new_key[:piece_count].reshape(piece_count, pairs_here, head_width),
            new_value[:piece_count].reshape(piece_count, pairs_here, head_width),
        ],
        axis=-1,
    )
    group_kv = jnp.concatenate([cache_kv, piece_kv], axis=0)
    group_bias = jnp.concatenate([cache_gate, new_bias], axis=1)
    my_group = lax.axis_index("kv")
    every_bias = lax.all_gather(group_bias, "kv", axis=1, tiled=True)
    own_query = query[:piece_count].reshape(piece_count, pairs_here, group_size, head_width)
    own_index = my_group * piece_count + jnp.arange(piece_count, dtype=jnp.int32)
    start_state = (
        jnp.full((piece_count, pairs_here, group_size), -jnp.inf, jnp.float32),
        jnp.zeros((piece_count, pairs_here, group_size), jnp.float32),
        jnp.zeros((piece_count, pairs_here, group_size, head_width), jnp.float32),
    )
    state = start_state
    piece = lax.all_gather(group_kv, "kv", axis=0, tiled=True)
    count = piece.shape[0] // group_rows
    blocks = piece.reshape(count, group_rows, pairs_here, 2 * head_width)

    def visit(carry, item):
        block, offset = item
        bias = lax.dynamic_slice_in_dim(every_bias, offset * group_rows, group_rows, 1)
        part = group_partial(
            own_query,
            own_index,
            block,
            bias.reshape(pairs_here, group_size, group_rows),
            offset,
            past_rows,
            piece_count,
        )
        return (merge_state(carry, part), None)

    state, _ = lax.scan(visit, state, (blocks, jnp.arange(count, dtype=jnp.int32)))
    peak, total, numer = state
    piece_attn = numer / total[..., None]
    dec_attn = decode_attention(
        query[piece_count:].reshape(dec_count, pairs_here, group_size, head_width),
        new_key[piece_count:].reshape(dec_count, pairs_here, head_width),
        new_value[piece_count:].reshape(dec_count, pairs_here, head_width),
        log_gate[piece_count:],
        dec_cache,
        dec_gate,
        dec_lengths,
    )
    attn_rows = jnp.concatenate(
        [
            piece_attn.reshape(piece_count, heads_here * head_width),
            dec_attn.reshape(dec_count, heads_here * head_width),
        ],
        axis=0,
    ).astype(jnp.bfloat16)
    every_head = lax.all_gather(attn_rows, "tp", axis=1, tiled=True)
    mixed = jnp.dot(every_head, w_out, preferred_element_type=jnp.float32).astype(jnp.bfloat16)
    return (mixed[:piece_count], mixed[piece_count:])


def solution(mesh):
    return jax.shard_map(
        local,
        mesh=mesh,
        in_specs=(
            P(("grp", "kv"), None),
            P(("grp", "kv"), None),
            P(),
            P(None, "tp"),
            P(None, "tp"),
            P(None, "tp"),
            P(None, "tp"),
            P("tp"),
            P("tp", ("grp", "kv")),
            P(("grp", "kv"), "tp", None),
            P("tp", ("grp", "kv")),
            P(("grp", "kv"), None, "tp", None),
            P(("grp", "kv"), "tp", None),
            P(("grp", "kv")),
            P(None, "tp"),
        ),
        out_specs=(P(("grp", "kv"), "tp"), P(("grp", "kv"), "tp")),
        check_vma=False,
    )
```

profile of v0, /device:TPU:0, one launch (start us, length us, event | category | flops | bytes accessed | tf_op | source)
XLA Modules:
  0.0 78.9 jit_solution(7893295334877088448)
XLA Ops:
  0.7 0.8 broadcast_add_fusion
  1.5 1.1 %fusion.35 = f32[66]{0:T(128)S(1)} fusion(bf16[2,2048]{1,0:T(2,128)(2,1)} %param.20, bf16[64,2048]{1,0:T(8,128)(2,1)} %param.19), kind=kLoop, calls=%fused_computation.54 | loop fusion | flops 810942 | bytes 270600 | tf_op jit(solution)/shard_map/reduce_sum | solution.py:22
  2.6 1.3 %fusion.42 = f32[66,4]{0,1:T(4,128)S(1)} fusion(bf16[2048,4]{0,1:T(4,128)(2,1)} %param.25, f32[4]{0:T(128)} %param.26, f32[2048]{0:T(1024)} %param.21, f32[66]{0:T(128)S(1)} %add_rsqrt_fusion, bf16[2,2048]{1,0:T(2,128)(2,1)} %param.20, bf16[64,2048]{1,0:T(8,128)(2,1)} %param.19), kind=kOutput, calls=%fused_computation.73 | convolution fusion | flops 2029896 | bytes 296248 | tf_op jit(solution)/shard_map/dot_general | solution.py:125
  3.9 0.7 bitcast_add_fusion
  4.7 1.0 %select_reduce_fusion = f32[2,4]{1,0:T(2,128)S(1)} fusion(f32[2,4,3072]{2,1,0:T(4,128)} %param.31, pred[2,3072]{1,0:T(4,128)(4,1)S(1)} %iota_compare_fusion.1), kind=kLoop, calls=%fused_computation.61 | loop fusion | flops 49144 | bytes 104480 | tf_op jit(solution)/shard_map/reduce_sum | solution.py:68
  5.8 0.7 iota_compare_fusion.2
  6.6 1.4 %convolution_convert_fusion.2 = bf16[66,64]{1,0:T(8,128)(2,1)S(1)} fusion(bf16[2048,64]{0,1:T(8,128)(2,1)} %param.24, f32[2048]{0:T(1024)} %param.21, f32[66]{0:T(128)S(1)} %add_rsqrt_fusion, bf16[2,2048]{1,0:T(2,128)(2,1)} %param.20, bf16[64,2048]{1,0:T(8,128)(2,1)} %param.19), kind=kOutput, calls=%fused_computation.45 | convolution fusion | flops 18251904 | bytes 549384 | tf_op jit(solution)/shard_map/dot_general | solution.py:123
  8.6 12.8 %all-gather = f32[4,1,4]{2,1,0:T(1,128)S(1)} all-gather(f32[1,1,4]{2,1,0:T(1,128)S(1)} %slice_bitcast_fusion.7), channel_id=1, replica_groups=mesh['grp'=2,'kv'=4,'tp'=4] {'kv'}, dimensions={0}, use_global_device_ids=true | all-gather | bytes 80 | tf_op jit(solution)/shard_map/all_gather | solution.py:9
  21.6 1.6 %convolution_convert_fusion.1 = bf16[66,256]{1,0:T(8,128)(2,1)S(1)} fusion(bf16[2048,256]{1,0:T(8,128)(2,1)} %param.22, f32[2048]{0:T(1024)S(1)} %copy-done.8, f32[66]{0:T(128)S(1)} %add_rsqrt_fusion, bf16[2,2048]{1,0:T(2,128)(2,1)S(1)} %copy-done.6, bf16[64,2048]{1,0:T(8,128)(2,1)S(1)} %copy-done.3), kind=kOutput, calls=%fused_computation.44 | convolution fusion | flops 70169088 | bytes 1361160 | tf_op jit(solution)/shard_map/dot_general | solution.py:121
  23.6 13.2 %all-gather.1 = f32[4,832,4]{1,2,0:T(4,128)S(1)} all-gather(f32[1,832,4]{1,2,0:T(4,128)S(1)} %maximum_bitcast_fusion), channel_id=1, replica_groups=mesh['grp'=2,'kv'=4,'tp'=4] {'kv'}, dimensions={0}, use_global_device_ids=true | all-gather | bytes 66560 | tf_op jit(solution)/shard_map/all_gather | solution.py:141
  36.9 0.6 fusion.53
  38.3 0.6 fusion.31
  39.2 17.8 %all_gather.12 = bf16[3328,1,128]{2,0,1:T(8,128)(2,1)S(1)} all-gather(bf16[832,1,128]{2,0,1:T(8,128)(2,1)S(1)} %maximum_maximum_fusion), channel_id=1, replica_groups=mesh['grp'=2,'kv'=4,'tp'=4] {'kv'}, dimensions={0}, use_global_device_ids=true | all-gather | bytes 1064960 | tf_op jit(solution)/shard_map/all_gather | solution.py:150
  57.0 14.4 %while.32 = (s32[]{:T(128)}, f32[64,1,4]{0,2,1:T(4,128)S(1)}, f32[64,1,4]{0,2,1:T(4,128)S(1)}, f32[64,1,4,64]{0,3,2,1:T(8,128)S(1)}, s32[4]{0:T(128)S(1)}, /*ind...) while((s32[]{:T(128)}, f32[64,1,4]{0,2,1:T(4,128)S(1)}, ...), condition=%wide.region_7.8_spmd.clone, body=%wide.region_4.7_spmd.clone.sunk | while | flops 56406536 | bytes 4148079 | solution.py:168
  57.0 0.6 dynamic_slice.41
  59.3 0.4 fusion.69
  59.7 0.3 fusion.71
  60.0 0.5 fusion.73
  60.6 0.6 dynamic_slice.41
  62.9 0.4 fusion.69
  63.3 0.3 fusion.71
  63.6 0.5 fusion.73
  64.2 0.6 dynamic_slice.41
  66.5 0.4 fusion.69
  67.3 0.5 fusion.73
  67.8 0.6 dynamic_slice.41
  70.1 0.4 fusion.69
  70.9 0.5 fusion.73
  71.5 5.8 %all_gather.15 = bf16[66,1024]{0,1:T(8,128)(2,1)S(1)} all-gather(bf16[66,256]{0,1:T(8,128)(2,1)S(1)} %pad_maximum_fusion.1), channel_id=1, replica_groups=mesh['grp'=2,'kv'=4,'tp'=4] {'tp'}, dimensions={1}, use_global_device_ids=true | all-gather | bytes 168960 | tf_op jit(solution)/shard_map/all_gather | solution.py:187
  77.3 0.3 convolution_convert_fusion
  77.7 0.6 slice.76
  78.3 0.6 slice.75
  (104 shorter events, 5.0 us)
Async XLA Ops:
  0.6 76.7 %copy-start = (bf16[1024,512]{1,0:T(8,128)(2,1)S(1)}, bf16[1024,512]{1,0:T(8,128)(2,1)}, u32[]{:S(2)}) copy-start(bf16[1024,512]{1,0:T(8,128)(2,1)} %param.33) | copy-start | bytes 3145732
  0.6 7.3 %copy-start.6 = (bf16[2,2048]{1,0:T(2,128)(2,1)S(1)}, bf16[2,2048]{1,0:T(2,128)(2,1)}, u32[]{:S(2)}) copy-start(bf16[2,2048]{1,0:T(2,128)(2,1)} %param.20) | copy-start | bytes 24580
  0.7 7.3 %copy-start.3 = (bf16[64,2048]{1,0:T(8,128)(2,1)S(1)}, bf16[64,2048]{1,0:T(8,128)(2,1)}, u32[]{:S(2)}) copy-start(bf16[64,2048]{1,0:T(8,128)(2,1)} %param.19) | copy-start | bytes 786436
  0.7 7.3 %copy-start.8 = (f32[2048]{0:T(1024)S(1)}, f32[2048]{0:T(1024)}, u32[]{:S(2)}) copy-start(f32[2048]{0:T(1024)} %param.21) | copy-start | bytes 24580
  0.7 7.3 %copy-start.7 = (bf16[2048,64]{0,1:T(8,128)(2,1)S(1)}, bf16[2048,64]{0,1:T(8,128)(2,1)}, u32[]{:S(2)}) copy-start(bf16[2048,64]{0,1:T(8,128)(2,1)} %param.23) | copy-start | bytes 786436
  2.6 18.9 %copy-start.5 = (f32[4,768]{1,0:T(4,128)S(1)}, f32[4,768]{1,0:T(4,128)}, u32[]{:S(2)}) copy-start(f32[4,768]{1,0:T(4,128)} %param.29) | copy-start | bytes 36868
  8.3 28.6 %copy-start.1 = (bf16[2,3072,1,128]{3,1,2,0:T(8,128)(2,1)S(1)}, bf16[2,3072,1,128]{3,1,2,0:T(8,128)(2,1)}, u32[]{:S(2)}) copy-start(bf16[2,3072,1,128]{3,1,2,0:T(8,128)(2,1)} %param.30) | copy-start | bytes 4718596
  8.3 28.6 %copy-start.2 = (f32[2,4,3072]{2,1,0:T(4,128)S(1)}, f32[2,4,3072]{2,1,0:T(4,128)}, u32[]{:S(2)}) copy-start(f32[2,4,3072]{2,1,0:T(4,128)} %param.31) | copy-start | bytes 294916
  36.9 2.2 %copy-start.4 = (bf16[768,1,128]{2,0,1:T(8,128)(2,1)S(1)}, bf16[768,1,128]{2,0,1:T(8,128)(2,1)}, u32[]{:S(2)}) copy-start(bf16[768,1,128]{2,0,1:T(8,128)(2,1)} %param.28) | copy-start | bytes 589828
where the time goes:
time: 79.3 us; the launch traced here: 78.9 us
  blocking collectives  49.5 us (62%)
  matrix products  9.82 us (12%)
  other arithmetic  6.95 us (9%)
  local copies, waits for them, and re-layouts  6.05 us (8%)
  loops' own time  5.61 us (7%)
  between operations  0.95 us (1%)
    all_gather x1, blocking collectives, local(): piece = lax.all_gather(group_kv, 'kv', axis=0, tiled=True)  17.8 us
    all_gather x1, blocking collectives, local(): every_bias = lax.all_gather(group_bias, 'kv', axis=1, tiled=True)  13.2 us
    all_gather x1, blocking collectives, carried_in(): everything = lax.all_gather(array, axis)  12.8 us
    all_gather x1, blocking collectives, local(): every_head = lax.all_gather(attn_rows, 'tp', axis=1, tiled=True)  5.78 us
    another operation x1, loops' own time, local(): lax.scan(visit, state, (blocks, jnp.arange(count, dtype=jnp.int32)))  5.54 us
    dynamic_slice x12, local copies, waits for them, and re-layouts, local(): lax.scan(visit, state, (blocks, jnp.arange(count, dtype=jnp.int32)))  3.1 us
    dot_general x4, matrix products, group_partial(): jnp.einsum('bkgn,nkd->bkgd', weight.astype(jnp.bfloat16), values, preferr...  2.11 us

commit v1 on v0

--- a/solution.py
+++ b/solution.py
@@ -184,7 +184,17 @@
         ],
         axis=0,
     ).astype(jnp.bfloat16)
-    every_head = lax.all_gather(attn_rows, "tp", axis=1, tiled=True)
+    n = lax.axis_size("tp")
+    series = [attn_rows]
+    h = 0
+    while h < n - 1:
+        series.append(
+            lax.ppermute(series[-1], axis_name="tp", perm=[(rr, (rr + 1) % n) for rr in range(n)])
+        )
+        h += 1
+    state_next = jnp.concatenate(series[::-1], 1)
+    tmp = lax.axis_index("tp")
+    every_head = jnp.roll(state_next, (tmp + 1) * attn_rows.shape[1], 1)
     mixed = jnp.dot(every_head, w_out, preferred_element_type=jnp.float32).astype(jnp.bfloat16)
     return (mixed[:piece_count], mixed[piece_count:])
 

time: 79.3 us -> 82.1 us (1.035)
  waiting for transfers between devices: 0 us -> 11.1 us
  blocking collectives: 49.5 us -> 43.6 us
  other arithmetic: 6.95 us -> 5.63 us
  matrix products: 9.82 us -> 8.67 us
    ppermute x0 -> x3, waiting for transfers between devices: none -> 11.1 us  [local(): lax.ppermute(series[-1], axis_name='tp', perm=[(rr, (rr + 1) % n) for rr...]
    all_gather x1 -> x0, blocking collectives: 5.78 us -> none  [local(): every_head = lax.all_gather(attn_rows, 'tp', axis=1, tiled=True)]
    dot_general x1, matrix products: 1.57 us -> 0.35 us  [local(): jnp.dot(normed, w_query, preferred_element_type=jnp.float32)]
    dot_general x1, matrix products: 0.3 us -> 1.36 us  [local(): jnp.dot(normed, w_key, preferred_element_type=jnp.float32)]
    dot_general x1, matrix products: 1.29 us -> 0.29 us  [local(): jnp.dot(normed, w_forget, preferred_element_type=jnp.float32) + forget_bias]
    reduce_sum x1, other arithmetic: 1.02 us -> 0.13 us  [decode_attention(): jnp.sum(jnp.where(target_location[None, None, :] == lengths[:, None, None...]
  transfers between devices with their start and end apart: 0 -> 3, of which waited for: 0 -> 3; matrix products, arithmetic and copies ran while one was open for 0% -> 0% of each run, Pallas kernels for 0% -> 0%
where the time goes in v1:
time: 82.1 us; the launch traced here: 81.8 us
  blocking collectives  43.6 us (53%)
  waiting for transfers between devices  11.1 us (14%)
  matrix products  8.67 us (11%)
  local copies, waits for them, and re-layouts  6.15 us (7%)
  other arithmetic  5.63 us (7%)
  loops' own time  5.61 us (7%)
  between operations  1.05 us (1%)
    all_gather x1, blocking collectives, local(): piece = lax.all_gather(group_kv, 'kv', axis=0, tiled=True)  17.8 us
    all_gather x1, blocking collectives, local(): every_bias = lax.all_gather(group_bias, 'kv', axis=1, tiled=True)  13.2 us
    all_gather x1, blocking collectives, carried_in(): everything = lax.all_gather(array, axis)  12.6 us
    ppermute x3, waiting for transfers between devices, local(): lax.ppermute(series[-1], axis_name='tp', perm=[(rr, (rr + 1) % n) for rr...  11.1 us
    another operation x1, loops' own time, local(): lax.scan(visit, state, (blocks, jnp.arange(count, dtype=jnp.int32)))  5.54 us
    dynamic_slice x12, local copies, waits for them, and re-layouts, local(): lax.scan(visit, state, (blocks, jnp.arange(count, dtype=jnp.int32)))  3.1 us
    dot_general x4, matrix products, group_partial(): jnp.einsum('bkgn,nkd->bkgd', weight.astype(jnp.bfloat16), values, preferr...  2.12 us
  transfers between devices with their start and end apart: 3, of which 3 were waited for; matrix products, arithmetic and copies ran while one was open for 0% of the time, Pallas kernels for 0%

profile of v1, /device:TPU:0, one launch (start us, length us, event | category | flops | bytes accessed | tf_op | source)
XLA Modules:
  0.0 81.8 jit_solution(10960877339099428022)
XLA Ops:
  0.7 0.8 broadcast_add_fusion
  1.5 0.7 iota_compare_fusion.2
  2.3 1.1 %fusion.35 = f32[66]{0:T(128)S(1)} fusion(bf16[2,2048]{1,0:T(2,128)(2,1)} %param.20, bf16[64,2048]{1,0:T(8,128)(2,1)} %param.19), kind=kLoop, calls=%fused_computation.54 | loop fusion | flops 810942 | bytes 270600 | tf_op jit(solution)/shard_map/reduce_sum | solution.py:22
  3.4 1.4 %convolution_convert_fusion.2 = bf16[66,64]{1,0:T(8,128)(2,1)S(1)} fusion(bf16[2048,64]{0,1:T(8,128)(2,1)} %param.24, f32[2048]{0:T(1024)} %param.21, f32[66]{0:T(128)S(1)} %add_rsqrt_fusion, bf16[2,2048]{1,0:T(2,128)(2,1)} %param.20, bf16[64,2048]{1,0:T(8,128)(2,1)} %param.19), kind=kOutput, calls=%fused_computation.45 | convolution fusion | flops 18251904 | bytes 549384 | tf_op jit(solution)/shard_map/dot_general | solution.py:123
  4.8 1.4 %convolution_convert_fusion.3 = bf16[66,64]{1,0:T(8,128)(2,1)S(1)} fusion(bf16[2048,64]{0,1:T(8,128)(2,1)} %param.23, f32[2048]{0:T(1024)} %param.21, f32[66]{0:T(128)S(1)} %add_rsqrt_fusion, bf16[2,2048]{1,0:T(2,128)(2,1)} %param.20, bf16[64,2048]{1,0:T(8,128)(2,1)} %param.19), kind=kOutput, calls=%fused_computation.46 | convolution fusion | flops 18251904 | bytes 549384 | tf_op jit(solution)/shard_map/dot_general | solution.py:122
  6.3 0.4 convolution_convert_fusion.1
  7.6 12.6 %all-gather = f32[4,1,4]{2,1,0:T(1,128)S(1)} all-gather(f32[1,1,4]{2,1,0:T(1,128)S(1)} %slice_bitcast_fusion.7), channel_id=1, replica_groups=mesh['grp'=2,'kv'=4,'tp'=4] {'kv'}, dimensions={0}, use_global_device_ids=true | all-gather | bytes 80 | tf_op jit(solution)/shard_map/all_gather | solution.py:9
  20.9 13.2 %all-gather.1 = f32[4,832,4]{1,2,0:T(4,128)S(1)} all-gather(f32[1,832,4]{1,2,0:T(4,128)S(1)} %maximum_bitcast_fusion), channel_id=1, replica_groups=mesh['grp'=2,'kv'=4,'tp'=4] {'kv'}, dimensions={0}, use_global_device_ids=true | all-gather | bytes 66560 | tf_op jit(solution)/shard_map/all_gather | solution.py:141
  34.2 0.6 fusion.55
  35.6 0.6 fusion.31
  36.4 17.8 %all_gather.9 = bf16[3328,1,128]{2,0,1:T(8,128)(2,1)S(1)} all-gather(bf16[832,1,128]{2,0,1:T(8,128)(2,1)S(1)} %maximum_maximum_fusion), channel_id=1, replica_groups=mesh['grp'=2,'kv'=4,'tp'=4] {'kv'}, dimensions={0}, use_global_device_ids=true | all-gather | bytes 1064960 | tf_op jit(solution)/shard_map/all_gather | solution.py:150
  54.2 14.4 %while.32 = (s32[]{:T(128)}, f32[64,1,4]{0,2,1:T(4,128)S(1)}, f32[64,1,4]{0,2,1:T(4,128)S(1)}, f32[64,1,4,64]{0,3,2,1:T(8,128)S(1)}, s32[4]{0:T(128)S(1)}, /*ind...) while((s32[]{:T(128)}, f32[64,1,4]{0,2,1:T(4,128)S(1)}, ...), condition=%wide.region_7.8_spmd.clone, body=%wide.region_4.7_spmd.clone.sunk | while | flops 56406536 | bytes 4148079 | solution.py:168
  54.2 0.6 dynamic_slice.48
  56.6 0.4 fusion.70
  56.9 0.3 fusion.72
  57.3 0.5 fusion.74
  57.9 0.6 dynamic_slice.48
  60.2 0.4 fusion.70
  60.6 0.3 fusion.72
  60.9 0.5 fusion.74
  61.5 0.6 dynamic_slice.48
  63.8 0.4 fusion.70
  64.5 0.5 fusion.74
  65.1 0.6 dynamic_slice.48
  67.4 0.4 fusion.70
  68.1 0.5 fusion.74
  68.9 3.7 %collective-permute-done = bf16[66,256]{0,1:T(8,128)(2,1)S(1)} collective-permute-done((bf16[66,256]{0,1:T(8,128)(2,1)S(1)}, bf16[66,256]{0,1:T(8,128)(2,1)S(1)}, u32[]{:S(2)}, u32[]{:S(2)}) %collective-permute-start) | collective-permute-done | bytes 33824 | tf_op jit(solution)/shard_map/ppermute | solution.py:192
  72.6 3.7 %collective-permute-done.1 = bf16[66,256]{0,1:T(8,128)(2,1)S(1)} collective-permute-done((bf16[66,256]{0,1:T(8,128)(2,1)S(1)}, bf16[66,256]{0,1:T(8,128)(2,1)S(1)}, u32[]{:S(2)}, u32[]{:S(2)}) %collective-permute-start.1) | collective-permute-done | bytes 33824 | tf_op jit(solution)/shard_map/ppermute | solution.py:192
  76.2 3.7 %collective-permute-done.2 = bf16[66,256]{0,1:T(8,128)(2,1)S(1)} collective-permute-done((bf16[66,256]{0,1:T(8,128)(2,1)S(1)}, bf16[66,256]{0,1:T(8,128)(2,1)S(1)}, u32[]{:S(2)}, u32[]{:S(2)}) %collective-permute-start.2) | collective-permute-done | bytes 33824 | tf_op jit(solution)/shard_map/ppermute | solution.py:192
  80.3 0.3 convolution_convert_fusion
  80.6 0.6 slice.76
  81.2 0.6 slice.75
  (123 shorter events, 5.5 us)
Async XLA Ops:
  0.6 79.6 %copy-start = (bf16[1024,512]{1,0:T(8,128)(2,1)S(1)}, bf16[1024,512]{1,0:T(8,128)(2,1)}, u32[]{:S(2)}) copy-start(bf16[1024,512]{1,0:T(8,128)(2,1)} %param.33) | copy-start | bytes 3145732
  0.6 5.6 %copy-start.6 = (bf16[2,2048]{1,0:T(2,128)(2,1)S(1)}, bf16[2,2048]{1,0:T(2,128)(2,1)}, u32[]{:S(2)}) copy-start(bf16[2,2048]{1,0:T(2,128)(2,1)} %param.20) | copy-start | bytes 24580
  0.7 5.6 %copy-start.3 = (bf16[64,2048]{1,0:T(8,128)(2,1)S(1)}, bf16[64,2048]{1,0:T(8,128)(2,1)}, u32[]{:S(2)}) copy-start(bf16[64,2048]{1,0:T(8,128)(2,1)} %param.19) | copy-start | bytes 786436
  0.7 5.6 %copy-start.10 = (f32[2048]{0:T(1024)S(1)}, f32[2048]{0:T(1024)}, u32[]{:S(2)}) copy-start(f32[2048]{0:T(1024)} %param.21) | copy-start | bytes 24580
  0.7 5.6 %copy-start.8 = (bf16[2048,256]{1,0:T(8,128)(2,1)S(1)}, bf16[2048,256]{1,0:T(8,128)(2,1)}, u32[]{:S(2)}) copy-start(bf16[2048,256]{1,0:T(8,128)(2,1)} %param.22) | copy-start | bytes 3145732
  4.8 2.0 %copy-start.9 = (bf16[2048,4]{0,1:T(4,128)(2,1)S(1)}, bf16[2048,4]{0,1:T(4,128)(2,1)}, u32[]{:S(2)}) copy-start(bf16[2048,4]{0,1:T(4,128)(2,1)} %param.25) | copy-start | bytes 49156
  4.8 2.0 %copy-start.11 = (f32[4]{0:T(128)S(1)}, f32[4]{0:T(128)}, u32[]{:S(2)}) copy-start(f32[4]{0:T(128)} %param.26) | copy-start | bytes 52
  4.8 2.3 %copy-start.7 = (f32[4,64]{1,0:T(4,128)S(1)}, f32[4,64]{1,0:T(4,128)}, u32[]{:S(2)}) copy-start(f32[4,64]{1,0:T(4,128)} %param.27) | copy-start | bytes 3076
  6.2 1.1 %copy-start.2 = (f32[2,4,3072]{2,1,0:T(4,128)S(1)}, f32[2,4,3072]{2,1,0:T(4,128)}, u32[]{:S(2)}) copy-start(f32[2,4,3072]{2,1,0:T(4,128)} %param.31) | copy-start | bytes 294916
  6.3 14.6 %copy-start.5 = (f32[4,768]{1,0:T(4,128)S(1)}, f32[4,768]{1,0:T(4,128)}, u32[]{:S(2)}) copy-start(f32[4,768]{1,0:T(4,128)} %param.29) | copy-start | bytes 36868
  6.3 27.9 %copy-start.1 = (bf16[2,3072,1,128]{3,1,2,0:T(8,128)(2,1)S(1)}, bf16[2,3072,1,128]{3,1,2,0:T(8,128)(2,1)}, u32[]{:S(2)}) copy-start(bf16[2,3072,1,128]{3,1,2,0:T(8,128)(2,1)} %param.30) | copy-start | bytes 4718596
  34.2 2.2 %copy-start.4 = (bf16[768,1,128]{2,0,1:T(8,128)(2,1)S(1)}, bf16[768,1,128]{2,0,1:T(8,128)(2,1)}, u32[]{:S(2)}) copy-start(bf16[768,1,128]{2,0,1:T(8,128)(2,1)} %param.28) | copy-start | bytes 589828
  68.8 3.7 %collective-permute-start = (bf16[66,256]{0,1:T(8,128)(2,1)S(1)}, bf16[66,256]{0,1:T(8,128)(2,1)S(1)}, u32[]{:S(2)}, u32[]{:S(2)}) collective-permute-start(bf16[66,256]{0,1:T(8,128)(2,1)S(1)} %pad_maximum_fusion.1), channel_id=1, source_target_pairs={{0,1},{1,2},{2,3},{3,0},{4,5},{5,6},{6,7},{7,4},{8,9},{9,10},{10,1... | collective-permute-start | bytes 101384 | tf_op jit(solution)/shard_map/ppermute | solution.py:192
  72.5 3.7 %collective-permute-start.1 = (bf16[66,256]{0,1:T(8,128)(2,1)S(1)}, bf16[66,256]{0,1:T(8,128)(2,1)S(1)}, u32[]{:S(2)}, u32[]{:S(2)}) collective-permute-start(bf16[66,256]{0,1:T(8,128)(2,1)S(1)} %collective-permute-done), channel_id=1, source_target_pairs={{0,1},{1,2},{2,3},{3,0},{4,5},{5,6},{6,7},{7,4},{8,9},{9,10},{10,1... | collective-permute-start | bytes 101384 | tf_op jit(solution)/shard_map/ppermute | solution.py:192
  76.2 3.7 %collective-permute-start.2 = (bf16[66,256]{0,1:T(8,128)(2,1)S(1)}, bf16[66,256]{0,1:T(8,128)(2,1)S(1)}, u32[]{:S(2)}, u32[]{:S(2)}) collective-permute-start(bf16[66,256]{0,1:T(8,128)(2,1)S(1)} %collective-permute-done.1), channel_id=1, source_target_pairs={{0,1},{1,2},{2,3},{3,0},{4,5},{5,6},{6,7},{7,4},{8,9},{9,10},{10,1... | collective-permute-start | bytes 101384 | tf_op jit(solution)/shard_map/ppermute | solution.py:192
